TPU v7x, 32 devices: a whole 2x2x4 slice. The times are simulated.
32 devices in a mesh: ep: 4 (over y, x), tp: 8 (over z, core).
Axes of the slice: x: 2, y: 2, z: 4, core: 2. Of those that a mesh axis runs over, the one named last changes fastest.
Arguments:
- mix_tokens: bfloat16 [4096, 2048], P(('ep', 'tp')), may hold values from -6 to 6
- mix_gain: bfloat16 [2048], replicated, may hold values from 0.099609375 to 1.8984375
- gate_proj: bfloat16 [2048, 1024], P(None, 'tp'), may hold values from -0.125 to 0.125
- conv_proj: bfloat16 [2048, 1024], P(None, 'tp'), may hold values from -0.125 to 0.125
- value_proj: bfloat16 [2048, 1024], P(None, 'tp'), may hold values from -0.125 to 0.125
- conv_taps: bfloat16 [3, 1024], P(None, 'tp'), may hold values from -3 to 3
- out_proj: bfloat16 [1024, 2048], P('tp'), may hold values from -0.1875 to 0.1875
- moe_tokens: bfloat16 [2048, 2048], P(('ep', 'tp')), may hold values from -6 to 6
- moe_gain: bfloat16 [2048], replicated, may hold values from 0.099609375 to 1.8984375
- expert_ids: int32 [2048, 2], P(('ep', 'tp')), may hold values from 0 to 3, all different within a row; in each aligned block of 64 rows (0 to 63, 64 to 127, ...) at most 36 rows name the same one
- expert_scores: float32 [2048, 2], P(('ep', 'tp')), may hold values from -6 to 6
- expert_gate: bfloat16 [4, 2048, 4096], P('ep', None, 'tp'), may hold values from -0.125 to 0.125
- expert_up: bfloat16 [4, 2048, 4096], P('ep', None, 'tp'), may hold values from -0.125 to 0.125
- expert_down: bfloat16 [4, 4096, 2048], P('ep', 'tp'), may hold values from -0.09375 to 0.09375
Outputs:
- mix_out: bfloat16 [4096, 2048], P(('ep', 'tp'))
- moe_out: bfloat16 [2048, 2048], P(('ep', 'tp'))
Inputs may be any that keep to these rules, and one draw needn't show every extreme that they name: `expert_ids`: each row names 2 different experts; among the rows of one device no expert is named more than 36 times.
All inputs are finite; a program needn't handle non-finite values.
Results may differ from a plain program's by a relative error of at most 0.018.
Values may be sent and summed in bfloat16 or wider, within the bound.
No kernel may reach another device: no remote copies, remote signals or barrier semaphores. Data moves between devices by JAX's collectives and lax.ppermute only.
A program may use at most 128 MiB of HBM per device.

v0:
```python
import jax
import jax.numpy as jnp
from jax import lax
from jax.sharding import PartitionSpec as P

norm_eps = 1e-06


def from_behind(value, axis, steps):
    count = lax.axis_size(axis)
    leading, last = (max(0, -steps), min(count, count - steps))
    return lax.ppermute(value, axis, [(source, source + steps) for source in range(leading, last)])


def scaled_norm(row_data, gain_vec):
    values = row_data.astype(jnp.float32)
    inverse = lax.rsqrt(jnp.mean(values * values, axis=1, keepdims=True) + norm_eps)
    return (values * inverse * gain_vec.astype(jnp.float32)).astype(jnp.bfloat16)


def shards(
    mix_tokens,
    mix_gain,
    gate_proj,
    conv_proj,
    value_proj,
    conv_taps,
    out_proj,
    moe_tokens,
    moe_gain,
    expert_ids,
    expert_scores,
    expert_gate,
    expert_up,
    expert_down,
):
    normed = scaled_norm(mix_tokens, mix_gain)
    w_joint = jnp.concatenate([gate_proj, conv_proj, value_proj], axis=1)
    combined = jnp.dot(
        lax.all_gather(normed, "tp", axis=0, tiled=True),
        w_joint,
        preferred_element_type=jnp.float32,
    ).astype(jnp.bfloat16)
    channels = gate_proj.shape[1]
    out_gate = combined[:, :channels]
    in_gate = combined[:, channels : 2 * channels]
    values = combined[:, 2 * channels :]
    signal = (in_gate.astype(jnp.float32) * values.astype(jnp.float32)).astype(jnp.bfloat16)
    tap_count = conv_taps.shape[0]
    before = from_behind(signal[signal.shape[0] - (tap_count - 1) :], "ep", 1)
    extended = jnp.concatenate([before, signal], axis=0)
    length = signal.shape[0]
    tap_values = conv_taps.astype(jnp.float32)
    convolved = jnp.zeros((length, channels), jnp.float32)
    for offset in range(tap_count):
        convolved = (
            convolved + extended[offset : offset + length].astype(jnp.float32) * tap_values[offset]
        )
    carried = (out_gate.astype(jnp.float32) * convolved).astype(jnp.bfloat16)
    row_block = carried
    mix_out = lax.psum_scatter(
        jnp.dot(row_block, out_proj, preferred_element_type=jnp.float32).astype(jnp.bfloat16),
        "tp",
        scatter_dimension=0,
        tiled=True,
    )
    moe_normed = scaled_norm(moe_tokens, moe_gain)
    experts = expert_gate.shape[0] * lax.axis_size("ep")
    row_count, top_count = expert_ids.shape
    capacity = top_count * row_count // experts + max(1, top_count * row_count // (8 * experts))
    width_model = moe_tokens.shape[1]
    flat_ids = expert_ids.reshape(-1)
    onehot = (flat_ids[:, None] == jnp.arange(experts, dtype=jnp.int32)[None, :]).astype(jnp.int32)
    slot_rank = jnp.sum((jnp.cumsum(onehot, axis=0) - onehot) * onehot, axis=1)
    slot_index = flat_ids * capacity + slot_rank
    slot_match = slot_index[:, None] == jnp.arange(experts * capacity, dtype=jnp.int32)[None, :]
    dispatch_map = jnp.any(
        slot_match.reshape(row_count, top_count, experts * capacity), axis=1
    ).astype(jnp.bfloat16)
    outgoing = lax.dot_general(
        dispatch_map, moe_normed, (((0,), (0,)), ((), ())), preferred_element_type=jnp.float32
    ).astype(jnp.bfloat16)
    arrived = lax.all_to_all(
        outgoing.reshape(experts, capacity, width_model),
        "ep",
        split_axis=0,
        concat_axis=0,
        tiled=True,
    )
    arrived_rows = arrived.reshape(-1, width_model)
    w_gate = expert_gate[0]
    w_up = expert_up[0]
    w_down = expert_down[0]
    portion = lax.all_gather(arrived_rows, "tp", axis=0, tiled=True)
    gate_value = jnp.dot(portion, w_gate, preferred_element_type=jnp.float32)
    up_value = jnp.dot(portion, w_up, preferred_element_type=jnp.float32)
    hidden = (jax.nn.silu(gate_value) * up_value).astype(jnp.bfloat16)
    row_block = hidden
    summed = lax.psum_scatter(
        jnp.dot(row_block, w_down, preferred_element_type=jnp.float32).astype(jnp.bfloat16),
        "tp",
        scatter_dimension=0,
        tiled=True,
    )
    returned = lax.all_to_all(
        summed.reshape(experts, capacity, width_model),
        "ep",
        split_axis=0,
        concat_axis=0,
        tiled=True,
    )
    flat_back = returned.reshape(experts * capacity, width_model)
    picked = flat_back[slot_index].reshape(row_count, top_count, width_model)
    route_weight = jax.nn.softmax(expert_scores, axis=1)
    moe_out = jnp.sum(route_weight[:, :, None] * picked.astype(jnp.float32), axis=1).astype(
        jnp.bfloat16
    )
    return (mix_out, moe_out)


def solution(mesh):
    in_specs = (
        P(("ep", "tp"), None),
        P(),
        P(None, "tp"),
        P(None, "tp"),
        P(None, "tp"),
        P(None, "tp"),
        P("tp", None),
        P(("ep", "tp"), None),
        P(),
        P(("ep", "tp"), None),
        P(("ep", "tp"), None),
        P("ep", None, "tp"),
        P("ep", None, "tp"),
        P("ep", "tp", None),
    )
    out_specs = (P(("ep", "tp"), None), P(("ep", "tp"), None))
    return jax.shard_map(shards, mesh=mesh, in_specs=in_specs, out_specs=out_specs, check_vma=False)
```

profile of v0, /device:TPU:0, one launch (start us, length us, event | category | flops | bytes accessed | tf_op | source)
XLA Modules:
  0.0 240.8 jit_solution(1236519495973544300)
XLA Ops:
  7.2 0.9 copy.23
  8.1 0.1 eq.29
  8.4 0.2 reduce_window_sum.11
  8.5 0.2 select_reduce_fusion
  8.7 0.1 reduce_sum.52
  9.1 0.7 convert_element_type.89
  9.8 1.1 fusion.19
  10.9 1.3 convolution_convert_fusion.2
  12.2 0.1 reshape.84
  12.4 14.9 %all_to_all.10 = bf16[4,36,2048]{2,1,0:T(8,128)(2,1)S(1)} all-to-all(bf16[4,36,2048]{2,1,0:T(8,128)(2,1)S(1)} %reshape.84), channel_id=1, replica_groups=mesh['ep'=4,'tp'=8] {'ep'}, dimensions={0} | all-to-all | bytes 1179648 | tf_op jit(solution)/shard_map/all_to_all | solution.py:83
  27.3 0.9 reshape.85
  28.3 1.2 fusion.14
  29.5 1.0 fusion.16
  30.6 48.7 %all-gather.5.cloned.1.call-done = bf16[1152,2048]{1,0:T(8,128)(2,1)} async-done(((bf16[144,2048]{1,0:T(8,128)(2,1)}), bf16[1152,2048]{1,0:T(8,128)(2,1)}) %all-gather.5.cloned.1.call-update) | async-done | bytes 4718608 | tf_op jit(solution)/shard_map/all_gather | solution.py:94
  79.3 7.0 %fusion.3 = f32[1152,512]{1,0:T(8,128)} fusion(bf16[1152,2048]{1,0:T(8,128)(2,1)} %all-gather.5.cloned.1.call-done, bf16[1,2048,512]{2,1,0:T(8,128)(2,1)} %param.25), kind=kOutput, calls=%fused_computation.8 | convolution fusion | flops 2415919104 | bytes 9175040 | tf_op jit(solution)/shard_map/dot_general | solution.py:95
  86.3 11.6 %convolution_convert_fusion = bf16[1152,2048]{1,0:T(8,128)(2,1)} fusion(bf16[1,512,2048]{2,1,0:T(8,128)(2,1)S(1)} %copy-done, bf16[1152,2048]{1,0:T(8,128)(2,1)} %all-gather.5.cloned.1.call-done, f32[1152,512]{1,0:T(8,128)} %fusion.3, bf16[1,2048,512]{2,1,0:T(8,128)(2,1)} %param.26), kind=kOutput, calls=%fused_computation.1 | convolution fusion | flops 4837736448 | bytes 15990784 | tf_op jit(solution)/shard_map/dot_general | solution.py:100
  98.0 0.6 copy-done.5
  98.6 28.5 %all-gather.3.cloned.1.call-done = bf16[1024,2048]{1,0:T(8,128)(2,1)} async-done(((bf16[128,2048]{1,0:T(8,128)(2,1)}), bf16[1024,2048]{1,0:T(8,128)(2,1)}) %all-gather.3.cloned.1.call-update) | async-done | bytes 4194320 | tf_op jit(solution)/shard_map/all_gather | solution.py:40
  127.1 4.8 %fusion.11 = bf16[1024,384]{1,0:T(8,128)(2,1)S(1)} fusion(bf16[1024,2048]{1,0:T(8,128)(2,1)} %all-gather.3.cloned.1.call-done, bf16[2048,128]{1,0:T(8,128)(2,1)S(1)} %copy-done.6, bf16[2048,128]{1,0:T(8,128)(2,1)} %param.17, bf16[2048,128]{1,0:T(8,128)(2,1)} %param.16), kind=kOutput, calls=%fused_computation.16 | convolution fusion | flops 1615724544 | bytes 6553600 | tf_op jit(solution)/shard_map/dot_general | solution.py:39
  132.0 3.4 %collective-permute-start = (bf16[2,128]{1,0:T(2,128)(2,1)S(1)}, bf16[2,128]{1,0:T(2,128)(2,1)S(1)}, u32[]{:S(2)}, u32[]{:S(2)}) collective-permute-start(bf16[2,128]{1,0:T(2,128)(2,1)S(1)} %slice.41), channel_id=1, source_target_pairs={{0,8},{8,16},{16,24},{1,9},{9,17},{17,25},{2,10},{10,18},{18,26},{... | collective-permute-start | bytes 1544 | tf_op jit(solution)/shard_map/ppermute | solution.py:12
  135.4 1.3 collective-permute-done
  136.7 3.3 %convolution_convert_fusion.1 = bf16[1024,2048]{1,0:T(8,128)(2,1)} fusion(bf16[128,2048]{1,0:T(8,128)(2,1)S(1)} %copy-done.2, bf16[1024,128]{1,0:T(8,128)(2,1)S(1)} %multiply_convert_fusion.1, bf16[2,128]{1,0:T(2,128)(2,1)S(1)} %collective-permute-done, bf16[1024,384]{1,0:T(8,128)(2,1)S(1)} %fusion.11, f32[128]{0:T(128)S(1)} %get-tuple-element.5, ...), kind=kOutput, calls=%fused_computation.2 | convolution fusion | flops 541196288 | bytes 5244928 | tf_op jit(solution)/shard_map/dot_general | solution.py:62
  140.0 0.7 copy-done.3
  140.7 42.5 %reduce-scatter.5.cloned.1.call-done = bf16[144,2048]{1,0:T(8,128)(2,1)} async-done(((bf16[1152,2048]{1,0:T(8,128)(2,1)}), bf16[144,2048]{1,0:T(8,128)(2,1)}) %reduce-scatter.5.cloned.1.call-update) | async-done | bytes 589840 | tf_op jit(solution)/shard_map/reduce_scatter | solution.py:99
  183.2 2.0 reshape.86
  185.2 3.7 %all-to-all-start.1 = ((bf16[4,36,2048]{2,1,0:T(8,128)(2,1)}), bf16[4,36,2048]{2,1,0:T(8,128)(2,1)S(1)}, u32[]{:S(2)}, u32[]{:S(2)}) async-start(bf16[4,36,2048]{2,1,0:T(8,128)(2,1)} %reshape.86), calls=%async_computation.3 | async-start | bytes 1310720 | tf_op jit(solution)/shard_map/all_to_all | solution.py:105
  188.9 0.1 mul.138
  189.1 7.4 %all-to-all-done.1 = bf16[4,36,2048]{2,1,0:T(8,128)(2,1)S(1)} async-done(((bf16[4,36,2048]{2,1,0:T(8,128)(2,1)}), bf16[4,36,2048]{2,1,0:T(8,128)(2,1)S(1)}, u32[]{:S(2)}, u32[]{:S(2)}) %all-to-all-start.1) | async-done | bytes 589856 | tf_op jit(solution)/shard_map/all_to_all | solution.py:105
  196.6 1.7 gather_fusion
  198.3 1.7 reshape.88
  200.1 2.2 multiply_reduce_fusion
  202.3 32.0 %reduce-scatter.3.cloned.1.call-done = bf16[128,2048]{1,0:T(8,128)(2,1)} async-done(((bf16[1024,2048]{1,0:T(8,128)(2,1)}), bf16[128,2048]{1,0:T(8,128)(2,1)}) %reduce-scatter.3.cloned.1.call-update) | async-done | bytes 524304 | tf_op jit(solution)/shard_map/reduce_scatter | solution.py:61
  (38 shorter events, 0.9 us)
Async XLA Ops:
  7.2 79.2 %copy-start = (bf16[1,512,2048]{2,1,0:T(8,128)(2,1)S(1)}, bf16[1,512,2048]{2,1,0:T(8,128)(2,1)}, u32[]{:S(2)}) copy-start(bf16[1,512,2048]{2,1,0:T(8,128)(2,1)} %param.27) | copy-start | bytes 6291460
  7.2 72.1 %all-gather.5.cloned.1.call-start = ((), (), s32[]{:S(2)}) async-start(), calls=%async_computation.6 | async-start | bytes 5308416 | tf_op jit(solution)/shard_map/all_gather | solution.py:94
  12.2 16.1 %copy-start.4 = (bf16[2048]{0:T(1024)(128)(2,1)S(1)}, bf16[2048]{0:T(1024)(128)(2,1)}, u32[]{:S(2)}) copy-start(bf16[2048]{0:T(1024)(128)(2,1)} %param.15) | copy-start | bytes 12292
  27.3 2.3 copy-start.1
  28.2 98.9 %all-gather.3.cloned.1.call-start = ((), (), s32[]{:S(2)}) async-start(), calls=%async_computation.4 | async-start | bytes 4718592 | tf_op jit(solution)/shard_map/all_gather | solution.py:40
  30.5 152.6 %reduce-scatter.5.cloned.1.call-start = ((), (), s32[]{:S(2)}) async-start(), calls=%async_computation.7 | async-start | bytes 5308416 | tf_op jit(solution)/shard_map/reduce_scatter | solution.py:99
  97.9 0.7 copy-start.5
  97.9 29.2 %copy-start.6 = (bf16[2048,128]{1,0:T(8,128)(2,1)S(1)}, bf16[2048,128]{1,0:T(8,128)(2,1)}, u32[]{:S(2)}) copy-start(bf16[2048,128]{1,0:T(8,128)(2,1)} %param.18) | copy-start | bytes 1572868
  98.0 136.4 %reduce-scatter.3.cloned.1.call-start = ((), (), s32[]{:S(2)}) async-start(), calls=%async_computation.5 | async-start | bytes 4718592 | tf_op jit(solution)/shard_map/reduce_scatter | solution.py:61
  98.6 38.1 %copy-start.2 = (bf16[128,2048]{1,0:T(8,128)(2,1)S(1)}, bf16[128,2048]{1,0:T(8,128)(2,1)}, u32[]{:S(2)}) copy-start(bf16[128,2048]{1,0:T(8,128)(2,1)} %param.20) | copy-start | bytes 1572868
  132.0 4.7 %collective-permute-start = (bf16[2,128]{1,0:T(2,128)(2,1)S(1)}, bf16[2,128]{1,0:T(2,128)(2,1)S(1)}, u32[]{:S(2)}, u32[]{:S(2)}) collective-permute-start(bf16[2,128]{1,0:T(2,128)(2,1)S(1)} %slice.41), channel_id=1, source_target_pairs={{0,8},{8,16},{16,24},{1,9},{9,17},{17,25},{2,10},{10,18},{18,26},{... | collective-permute-start | bytes 1544 | tf_op jit(solution)/shard_map/ppermute | solution.py:12
  140.0 0.7 copy-start.3
  185.2 11.3 %all-to-all-start.1 = ((bf16[4,36,2048]{2,1,0:T(8,128)(2,1)}), bf16[4,36,2048]{2,1,0:T(8,128)(2,1)S(1)}, u32[]{:S(2)}, u32[]{:S(2)}) async-start(bf16[4,36,2048]{2,1,0:T(8,128)(2,1)} %reshape.86), calls=%async_computation.3 | async-start | bytes 1310720 | tf_op jit(solution)/shard_map/all_to_all | solution.py:105
Sparse Core Ops, SparseCore 0:
  28.3 50.9 all-gather.4
  81.5 45.6 all-gather.2
  129.4 53.6 reduce-scatter.4
  185.9 48.3 reduce-scatter.2
where the time goes:
time: 241 us
  waiting for transfers between devices  160 us (66%)
  matrix products  28 us (12%)
  blocking collectives  14.9 us (6%)
  between operations  13.9 us (6%)
  local copies, waits for them, and re-layouts  9.37 us (4%)
  starting transfers between devices  7.19 us (3%)
  other arithmetic  6.94 us (3%)
    all_gather x1, waiting for transfers between devices, shards(): portion = lax.all_gather(arrived_rows, 'tp', axis=0, tiled=True)  48.7 us
    reduce_scatter x1, waiting for transfers between devices, shards(): lax.psum_scatter(jnp.dot(row_block, w_down, preferred_element_type=jnp.fl...  42.5 us
    reduce_scatter x1, waiting for transfers between devices, shards(): lax.psum_scatter(jnp.dot(row_block, out_proj, preferred_element_type=jnp....  32 us
    all_gather x1, waiting for transfers between devices, shards(): lax.all_gather(normed, 'tp', axis=0, tiled=True)  28.5 us
    all_to_all x1, blocking collectives, shards(): lax.all_to_all(outgoing.reshape(experts, capacity, width_model), 'ep', sp...  14.9 us
    dot_general x1, matrix products, shards(): jnp.dot(row_block, w_down, preferred_element_type=jnp.float32)  11.6 us
    all_to_all x1, waiting for transfers between devices, shards(): lax.all_to_all(summed.reshape(experts, capacity, width_model), 'ep', spli...  7.39 us
    dot_general x1, matrix products, shards(): gate_value = jnp.dot(portion, w_gate, preferred_element_type=jnp.float32)  7.02 us
  transfers between devices with their start and end apart: 6, of which 6 were waited for; matrix products, arithmetic and copies ran while one was open for 15% of the time, Pallas kernels for 0%

commit v1 on v0

--- a/solution.py
+++ b/solution.py
@@ -4,12 +4,6 @@
 from jax.sharding import PartitionSpec as P
 
 norm_eps = 1e-06
-
-
-def from_behind(value, axis, steps):
-    count = lax.axis_size(axis)
-    leading, last = (max(0, -steps), min(count, count - steps))
-    return lax.ppermute(value, axis, [(source, source + steps) for source in range(leading, last)])
 
 
 def scaled_norm(row_data, gain_vec):
@@ -34,37 +28,40 @@
     expert_up,
     expert_down,
 ):
+    n_ep = lax.axis_size("ep")
+    n_tp = lax.axis_size("tp")
+    half = n_tp // 2
+    ep_index = lax.axis_index("ep")
+    channels = gate_proj.shape[1]
+    halves = [list(range(half)), list(range(half, n_tp))]
+    joint = jnp.concatenate([gate_proj, conv_proj, value_proj], axis=1)
+    swap = [(t, t ^ half) for t in range(n_tp)]
+
+    def own_piece(array):
+        rows = array.shape[0] // n_ep
+        return lax.ppermute(
+            lax.dynamic_slice_in_dim(array, ep_index * rows, rows, 0), "tp", swap
+        )
+
+    def assembled(piece, array):
+        rows = array.shape[0] // n_ep
+        whole = lax.dynamic_update_slice_in_dim(
+            jnp.zeros_like(array), piece, ep_index * rows, 0
+        )
+        for k in range(1, n_ep):
+            arrived_piece = lax.ppermute(piece, "ep", [(e, e ^ k) for e in range(n_ep)])
+            whole = lax.dynamic_update_slice_in_dim(
+                whole, arrived_piece, (ep_index ^ k) * rows, 0
+            )
+        return whole
+
+    joint_piece = own_piece(joint)
+    out_piece = own_piece(out_proj)
+    other_taps = lax.ppermute(conv_taps, "tp", swap)
     normed = scaled_norm(mix_tokens, mix_gain)
-    w_joint = jnp.concatenate([gate_proj, conv_proj, value_proj], axis=1)
-    combined = jnp.dot(
-        lax.all_gather(normed, "tp", axis=0, tiled=True),
-        w_joint,
-        preferred_element_type=jnp.float32,
-    ).astype(jnp.bfloat16)
-    channels = gate_proj.shape[1]
-    out_gate = combined[:, :channels]
-    in_gate = combined[:, channels : 2 * channels]
-    values = combined[:, 2 * channels :]
-    signal = (in_gate.astype(jnp.float32) * values.astype(jnp.float32)).astype(jnp.bfloat16)
-    tap_count = conv_taps.shape[0]
-    before = from_behind(signal[signal.shape[0] - (tap_count - 1) :], "ep", 1)
-    extended = jnp.concatenate([before, signal], axis=0)
-    length = signal.shape[0]
-    tap_values = conv_taps.astype(jnp.float32)
-    convolved = jnp.zeros((length, channels), jnp.float32)
-    for offset in range(tap_count):
-        convolved = (
-            convolved + extended[offset : offset + length].astype(jnp.float32) * tap_values[offset]
-        )
-    carried = (out_gate.astype(jnp.float32) * convolved).astype(jnp.bfloat16)
-    row_block = carried
-    mix_out = lax.psum_scatter(
-        jnp.dot(row_block, out_proj, preferred_element_type=jnp.float32).astype(jnp.bfloat16),
-        "tp",
-        scatter_dimension=0,
-        tiled=True,
-    )
     moe_normed = scaled_norm(moe_tokens, moe_gain)
+    normed, moe_normed = lax.optimization_barrier((normed, moe_normed))
+    gathered = lax.all_gather(normed, "tp", axis=0, tiled=True, axis_index_groups=halves)
     experts = expert_gate.shape[0] * lax.axis_size("ep")
     row_count, top_count = expert_ids.shape
     capacity = top_count * row_count // experts + max(1, top_count * row_count // (8 * experts))
@@ -88,20 +85,57 @@
         tiled=True,
     )
     arrived_rows = arrived.reshape(-1, width_model)
+    arrived_rows, gathered, joint_piece, out_piece, other_taps = lax.optimization_barrier(
+        (arrived_rows, gathered, joint_piece, out_piece, other_taps)
+    )
+    portion = lax.all_gather(arrived_rows, "tp", axis=0, tiled=True)
+    other_joint = assembled(joint_piece, joint)
+    other_out = assembled(out_piece, out_proj)
+    own_values = jnp.dot(gathered, joint, preferred_element_type=jnp.float32).astype(jnp.bfloat16)
+    other_values = jnp.dot(gathered, other_joint, preferred_element_type=jnp.float32).astype(
+        jnp.bfloat16
+    )
+    out_gate, in_gate, values = (
+        jnp.concatenate(
+            [part[:, index * channels : (index + 1) * channels] for part in (own_values, other_values)],
+            axis=1,
+        )
+        for index in range(3)
+    )
+    signal = (in_gate.astype(jnp.float32) * values.astype(jnp.float32)).astype(jnp.bfloat16)
+    tap_count = conv_taps.shape[0]
+    length = signal.shape[0]
+    tail = signal[length - (tap_count - 1) :]
+    tail = jnp.concatenate([tail[:, channels:], tail[:, :channels]], axis=1)
+    steps = [
+        (device, device + half) for device in range(n_ep * n_tp - half)
+    ]
+    before = lax.ppermute(tail, ("ep", "tp"), steps)
+    extended = jnp.concatenate([before, signal], axis=0)
+    tap_values = jnp.concatenate([conv_taps, other_taps], axis=1).astype(jnp.float32)
+    convolved = jnp.zeros((length, 2 * channels), jnp.float32)
+    for offset in range(tap_count):
+        convolved = (
+            convolved + extended[offset : offset + length].astype(jnp.float32) * tap_values[offset]
+        )
+    carried = (out_gate.astype(jnp.float32) * convolved).astype(jnp.bfloat16)
+    out_weights = jnp.concatenate([out_proj, other_out], axis=0)
+    mix_partial = jnp.dot(carried, out_weights, preferred_element_type=jnp.float32).astype(
+        jnp.bfloat16
+    )
+    portion, mix_partial = lax.optimization_barrier((portion, mix_partial))
+    mix_out = lax.psum_scatter(
+        mix_partial, "tp", scatter_dimension=0, tiled=True, axis_index_groups=halves
+    )
     w_gate = expert_gate[0]
     w_up = expert_up[0]
     w_down = expert_down[0]
-    portion = lax.all_gather(arrived_rows, "tp", axis=0, tiled=True)
     gate_value = jnp.dot(portion, w_gate, preferred_element_type=jnp.float32)
     up_value = jnp.dot(portion, w_up, preferred_element_type=jnp.float32)
     hidden = (jax.nn.silu(gate_value) * up_value).astype(jnp.bfloat16)
-    row_block = hidden
-    summed = lax.psum_scatter(
-        jnp.dot(row_block, w_down, preferred_element_type=jnp.float32).astype(jnp.bfloat16),
-        "tp",
-        scatter_dimension=0,
-        tiled=True,
-    )
+    moe_partial = jnp.dot(hidden, w_down, preferred_element_type=jnp.float32).astype(jnp.bfloat16)
+    moe_partial, mix_out = lax.optimization_barrier((moe_partial, mix_out))
+    summed = lax.psum_scatter(moe_partial, "tp", scatter_dimension=0, tiled=True)
     returned = lax.all_to_all(
         summed.reshape(experts, capacity, width_model),
         "ep",

time: 241 us -> 221 us (0.917)
  waiting for transfers between devices: 160 us -> 130 us
  starting transfers between devices: 7.19 us -> 26.4 us
  blocking collectives: 14.9 us -> 0 us
  local copies, waits for them, and re-layouts: 9.37 us -> 14.1 us
  other arithmetic: 6.94 us -> 10.5 us
  matrix products: 28 us -> 25.5 us
    ppermute x1 -> x10, waiting for transfers between devices: 1.27 us -> 36.3 us  [the longest x1 17.8 us: shards(): other_taps = lax.ppermute(conv_taps, 'tp', swap)]
    all_gather x1, waiting for transfers between devices: 48.7 us -> 16.8 us  [shards(): portion = lax.all_gather(arrived_rows, 'tp', axis=0, tiled=True)]
    all_gather x1, waiting for transfers between devices: 28.5 us -> 3.5 us  [shards(): lax.all_gather(normed, 'tp', axis=0, tiled=True, axis_index_groups=halves)]
    all_to_all x1 -> x0, blocking collectives: 14.9 us -> none  [shards(): lax.all_to_all(outgoing.reshape(experts, capacity, width_model), 'ep', sp...]
    ppermute x1 -> x10, starting transfers between devices: 3.37 us -> 17.2 us  [the longest x6 7.32 us: assembled(): arrived_piece = lax.ppermute(piece, 'ep', [(e, e ^ k) for e in range(n_ep)])]
    reduce_scatter x2, waiting for transfers between devices: 74.5 us -> 65.7 us  [the longest x1 57 us: shards(): lax.psum_scatter(moe_partial, 'tp', scatter_dimension=0, tiled=True)]
    all_to_all x0 -> x1, starting transfers between devices: none -> 5.19 us  [shards(): lax.all_to_all(outgoing.reshape(experts, capacity, width_model), 'ep', sp...]
    dot_general x3 -> x4, matrix products: 19.7 us -> 18.1 us  [the longest x1 11.2 us: shards(): jnp.dot(hidden, w_down, preferred_element_type=jnp.float32)]
  transfers between devices with their start and end apart: 6 -> 16, of which waited for: 6 -> 8; matrix products, arithmetic and copies ran while one was open for 15% -> 15% of each run, Pallas kernels for 0% -> 0%
where the time goes in v1:
time: 221 us; the launch traced here: 220 us
  waiting for transfers between devices  130 us (59%)
  starting transfers between devices  26.4 us (12%)
  matrix products  25.5 us (12%)
  between operations  14.2 us (6%)
  local copies, waits for them, and re-layouts  14.1 us (6%)
  other arithmetic  10.5 us (5%)
    reduce_scatter x1, waiting for transfers between devices, shards(): lax.psum_scatter(moe_partial, 'tp', scatter_dimension=0, tiled=True)  57 us
    ppermute x1, waiting for transfers between devices, shards(): other_taps = lax.ppermute(conv_taps, 'tp', swap)  17.8 us
    all_gather x1, waiting for transfers between devices, shards(): portion = lax.all_gather(arrived_rows, 'tp', axis=0, tiled=True)  16.8 us
    ppermute x6, waiting for transfers between devices, assembled(): arrived_piece = lax.ppermute(piece, 'ep', [(e, e ^ k) for e in range(n_ep)])  15 us
    dot_general x1, matrix products, shards(): jnp.dot(hidden, w_down, preferred_element_type=jnp.float32)  11.2 us
    reduce_scatter x1, waiting for transfers between devices, shards(): lax.psum_scatter(mix_partial, 'tp', scatter_dimension=0, tiled=True, axis...  8.72 us
    all_to_all x1, waiting for transfers between devices, shards(): lax.all_to_all(summed.reshape(experts, capacity, width_model), 'ep', spli...  7.39 us
    ppermute x6, starting transfers between devices, assembled(): arrived_piece = lax.ppermute(piece, 'ep', [(e, e ^ k) for e in range(n_ep)])  7.32 us
  transfers between devices with their start and end apart: 16, of which 8 were waited for; matrix products, arithmetic and copies ran while one was open for 15% of the time, Pallas kernels for 0%

profile of v1, /device:TPU:0, one launch (start us, length us, event | category | flops | bytes accessed | tf_op | source)
XLA Modules:
  0.0 220.4 jit_solution(3129712093656413787)
XLA Ops:
  7.2 1.4 fusion.5
  8.6 1.1 fusion.13
  11.1 1.1 fusion.15
  12.2 2.0 fusion.7
  17.2 5.2 %all-to-all-start = ((bf16[4,36,2048]{2,1,0:T(8,128)(2,1)}), bf16[4,36,2048]{2,1,0:T(8,128)(2,1)S(1)}, u32[]{:S(2)}, u32[]{:S(2)}) async-start(bf16[4,36,2048]{2,1,0:T(8,128)(2,1)} %reshape.84), calls=%async_computation | async-start | bytes 1310720 | tf_op jit(solution)/shard_map/all_to_all | solution.py:80
  22.5 1.3 constant_dynamic-update-slice_fusion.1
  24.0 1.2 copy-done.1
  25.2 2.7 %collective-permute-start = (bf16[512,384]{1,0:T(8,128)(2,1)S(1)}, bf16[512,384]{1,0:T(8,128)(2,1)S(1)}, u32[]{:S(2)}, u32[]{:S(2)}) collective-permute-start(bf16[512,384]{1,0:T(8,128)(2,1)S(1)} %constant_dynamic-slice_fusion.1), channel_id=1, source_target_pairs={{0,4},{1,5},{2,6},{3,7},{4,0},{5,1},{6,2},{7,3},{8,12},{9,13},{10,... | collective-permute-start | bytes 1179656 | tf_op jit(solution)/shard_map/ppermute | solution.py:42
  27.8 1.6 constant_dynamic-slice_fusion
  29.8 2.6 %collective-permute-start.2 = (bf16[3,128]{1,0:T(4,128)(2,1)S(1)}, bf16[3,128]{1,0:T(4,128)(2,1)S(1)}, u32[]{:S(2)}, u32[]{:S(2)}) collective-permute-start(bf16[3,128]{1,0:T(4,128)(2,1)S(1)} %copy-done.8), channel_id=1, source_target_pairs={{0,4},{1,5},{2,6},{3,7},{4,0},{5,1},{6,2},{7,3},{8,12},{9,13},{10,... | collective-permute-start | bytes 2312 | tf_op jit(solution)/shard_map/ppermute | solution.py:60
  32.3 1.0 reshape.85
  33.3 17.8 %collective-permute-done.2 = bf16[3,128]{1,0:T(4,128)(2,1)S(1)} collective-permute-done((bf16[3,128]{1,0:T(4,128)(2,1)S(1)}, bf16[3,128]{1,0:T(4,128)(2,1)S(1)}, u32[]{:S(2)}, u32[]{:S(2)}) %collective-permute-start.2) | collective-permute-done | bytes 800 | tf_op jit(solution)/shard_map/ppermute | solution.py:60
  51.1 3.5 %all-gather.3.cloned.1.call-done = bf16[512,2048]{1,0:T(8,128)(2,1)} async-done(((bf16[128,2048]{1,0:T(8,128)(2,1)}), bf16[512,2048]{1,0:T(8,128)(2,1)}) %all-gather.3.cloned.1.call-update) | async-done | bytes 2097168 | tf_op jit(solution)/shard_map/all_gather | solution.py:64
  54.7 2.4 %collective-permute-start.9 = (bf16[32,2048]{1,0:T(8,128)(2,1)}, bf16[32,2048]{1,0:T(8,128)(2,1)S(1)}, u32[]{:S(2)}, u32[]{:S(2)}) collective-permute-start(bf16[32,2048]{1,0:T(8,128)(2,1)} %collective-permute-done.1), channel_id=1, source_target_pairs={{0,24},{8,16},{16,8},{24,0},{1,25},{9,17},{17,9},{25,1},{2,26},{10... | collective-permute-start | bytes 393224 | tf_op jit(solution)/shard_map/ppermute | solution.py:52
  58.3 2.4 %collective-permute-start.5 = (bf16[512,384]{1,0:T(8,128)(2,1)S(1)}, bf16[512,384]{1,0:T(8,128)(2,1)S(1)}, u32[]{:S(2)}, u32[]{:S(2)}) collective-permute-start(bf16[512,384]{1,0:T(8,128)(2,1)S(1)} %collective-permute-done), channel_id=1, source_target_pairs={{0,24},{8,16},{16,8},{24,0},{1,25},{9,17},{17,9},{25,1},{2,26},{10... | collective-permute-start | bytes 1179656 | tf_op jit(solution)/shard_map/ppermute | solution.py:52
  62.2 3.3 %convolution_convert_fusion.4 = bf16[512,384]{0,1:T(8,128)(2,1)S(1)} fusion(bf16[512,2048]{1,0:T(8,128)(2,1)} %all-gather.3.cloned.1.call-done, bf16[2048,384]{1,0:T(8,128)(2,1)} %copy-done.1), kind=kOutput, calls=%fused_computation.13 | convolution fusion | flops 805502976 | bytes 4063232 | tf_op jit(solution)/shard_map/dot_general | solution.py:94
  66.7 15.0 %collective-permute-done.3 = bf16[512,384]{1,0:T(8,128)(2,1)S(1)} collective-permute-done((bf16[512,384]{1,0:T(8,128)(2,1)S(1)}, bf16[512,384]{1,0:T(8,128)(2,1)S(1)}, u32[]{:S(2)}, u32[]{:S(2)}) %collective-permute-start.3) | collective-permute-done | bytes 393248 | tf_op jit(solution)/shard_map/ppermute | solution.py:52
  81.9 1.0 convolution_convert_fusion.3
  83.2 4.3 %collective-permute-start.6 = (bf16[2,256]{0,1:T(8,128)(2,1)S(1)}, bf16[2,256]{0,1:T(8,128)(2,1)S(1)}, u32[]{:S(2)}, u32[]{:S(2)}) collective-permute-start(bf16[2,256]{0,1:T(8,128)(2,1)S(1)} %pad_maximum_fusion.2), channel_id=1, source_target_pairs={{0,4},{1,5},{2,6},{3,7},{4,8},{5,9},{6,10},{7,11},{8,12},{9,13},{1... | collective-permute-start | bytes 3080 | tf_op jit(solution)/shard_map/ppermute | solution.py:113
  87.6 3.5 %collective-permute-done.6 = bf16[2,256]{0,1:T(8,128)(2,1)S(1)} collective-permute-done((bf16[2,256]{0,1:T(8,128)(2,1)S(1)}, bf16[2,256]{0,1:T(8,128)(2,1)S(1)}, u32[]{:S(2)}, u32[]{:S(2)}) %collective-permute-start.6) | collective-permute-done | bytes 1056 | tf_op jit(solution)/shard_map/ppermute | solution.py:113
  91.1 2.6 %convolution_convert_fusion.1 = bf16[512,2048]{1,0:T(8,128)(2,1)} fusion(bf16[128,2048]{1,0:T(8,128)(2,1)S(1)} %constant_dynamic-update-slice_fusion.3, bf16[128,2048]{1,0:T(8,128)(2,1)S(1)} %copy-done.5, bf16[512,256]{0,1:T(8,128)(2,1)S(1)} %multiply_convert_fusion.1, bf16[2,256]{0,1:T(8,128)(2,1)S(1)} %collective-permute-done.6, ...), kind=kOutput, calls=%fused_computation.3 | convolution fusion | flops 542638080 | bytes 3674112 | tf_op jit(solution)/shard_map/dot_general | solution.py:123
  93.7 16.8 %all-gather.5.cloned.1.call-done = bf16[1152,2048]{1,0:T(8,128)(2,1)} async-done(((bf16[144,2048]{1,0:T(8,128)(2,1)}), bf16[1152,2048]{1,0:T(8,128)(2,1)}) %all-gather.5.cloned.1.call-update) | async-done | bytes 4718608 | tf_op jit(solution)/shard_map/all_gather | solution.py:91
  110.8 7.0 %fusion.3 = f32[1152,512]{1,0:T(8,128)} fusion(bf16[1152,2048]{1,0:T(8,128)(2,1)} %all-gather.5.cloned.1.call-done, bf16[1,2048,512]{2,1,0:T(8,128)(2,1)} %param.25), kind=kOutput, calls=%fused_computation.8 | convolution fusion | flops 2415919104 | bytes 9175040 | tf_op jit(solution)/shard_map/dot_general | solution.py:133
  117.8 11.2 %convolution_convert_fusion = bf16[1152,2048]{1,0:T(8,128)(2,1)} fusion(bf16[1,512,2048]{2,1,0:T(8,128)(2,1)S(1)} %copy-done, bf16[1152,2048]{1,0:T(8,128)(2,1)} %all-gather.5.cloned.1.call-done, f32[1152,512]{1,0:T(8,128)} %fusion.3, bf16[1,2048,512]{2,1,0:T(8,128)(2,1)} %param.26), kind=kOutput, calls=%fused_computation.1 | convolution fusion | flops 4837736448 | bytes 15990784 | tf_op jit(solution)/shard_map/dot_general | solution.py:136
  129.0 8.7 %reduce-scatter.3.cloned.1.call-done = bf16[128,2048]{1,0:T(8,128)(2,1)} async-done(((bf16[512,2048]{1,0:T(8,128)(2,1)}), bf16[128,2048]{1,0:T(8,128)(2,1)}) %reduce-scatter.3.cloned.1.call-update) | async-done | bytes 524304 | tf_op jit(solution)/shard_map/reduce_scatter | solution.py:127
  137.8 57.0 %reduce-scatter.5.cloned.1.call-done = bf16[144,2048]{1,0:T(8,128)(2,1)} async-done(((bf16[1152,2048]{1,0:T(8,128)(2,1)}), bf16[144,2048]{1,0:T(8,128)(2,1)}) %reduce-scatter.5.cloned.1.call-update) | async-done | bytes 589840 | tf_op jit(solution)/shard_map/reduce_scatter | solution.py:138
  194.8 2.0 reshape.86
  196.8 3.7 %all-to-all-start.1 = ((bf16[4,36,2048]{2,1,0:T(8,128)(2,1)}), bf16[4,36,2048]{2,1,0:T(8,128)(2,1)S(1)}, u32[]{:S(2)}, u32[]{:S(2)}) async-start(bf16[4,36,2048]{2,1,0:T(8,128)(2,1)} %reshape.86), calls=%async_computation.3 | async-start | bytes 1310720 | tf_op jit(solution)/shard_map/all_to_all | solution.py:139
  200.7 7.4 %all-to-all-done.1 = bf16[4,36,2048]{2,1,0:T(8,128)(2,1)S(1)} async-done(((bf16[4,36,2048]{2,1,0:T(8,128)(2,1)}), bf16[4,36,2048]{2,1,0:T(8,128)(2,1)S(1)}, u32[]{:S(2)}, u32[]{:S(2)}) %all-to-all-start.1) | async-done | bytes 589856 | tf_op jit(solution)/shard_map/all_to_all | solution.py:139
  208.2 1.7 gather_fusion
  210.0 1.7 reshape.88
  211.6 2.2 %multiply_reduce_fusion = bf16[64,2048]{1,0:T(8,128)(2,1)} fusion(f32[64,2,2048]{2,1,0:T(2,128)S(1)} %reshape.88, f32[64,2]{1,0:T(8,128)S(1)} %copy.31), kind=kLoop, calls=%fused_computation.20 | loop fusion | flops 393216 | bytes 1311232 | tf_op jit(solution)/shard_map/reduce_sum | solution.py:149
  (81 shorter events, 9.9 us)
Async XLA Ops:
  7.2 110.7 %copy-start = (bf16[1,512,2048]{2,1,0:T(8,128)(2,1)S(1)}, bf16[1,512,2048]{2,1,0:T(8,128)(2,1)}, u32[]{:S(2)}) copy-start(bf16[1,512,2048]{2,1,0:T(8,128)(2,1)} %param.27) | copy-start | bytes 6291460
  7.2 7.1 %copy-start.7 = (s32[64,2]{0,1:T(2,128)S(1)}, s32[64,2]{0,1:T(2,128)}, u32[]{:S(2)}) copy-start(s32[64,2]{0,1:T(2,128)} %param.23) | copy-start | bytes 1540
  7.2 47.4 %all-gather.3.cloned.1.call-start = ((), (), s32[]{:S(2)}) async-start(), calls=%async_computation.4 | async-start | bytes 2621440 | tf_op jit(solution)/shard_map/all_gather | solution.py:64
  14.3 8.2 %copy-start.2 = (bf16[2048,128]{1,0:T(8,128)(2,1)S(1)}, bf16[2048,128]{1,0:T(8,128)(2,1)}, u32[]{:S(2)}) copy-start(bf16[2048,128]{1,0:T(8,128)(2,1)} %param.16) | copy-start | bytes 1572868
  17.2 15.1 %all-to-all-start = ((bf16[4,36,2048]{2,1,0:T(8,128)(2,1)}), bf16[4,36,2048]{2,1,0:T(8,128)(2,1)S(1)}, u32[]{:S(2)}, u32[]{:S(2)}) async-start(bf16[4,36,2048]{2,1,0:T(8,128)(2,1)} %reshape.84), calls=%async_computation | async-start | bytes 1310720 | tf_op jit(solution)/shard_map/all_to_all | solution.py:80
  22.4 88.1 %all-gather.5.cloned.1.call-start = ((), (), s32[]{:S(2)}) async-start(), calls=%async_computation.5 | async-start | bytes 5308416 | tf_op jit(solution)/shard_map/all_gather | solution.py:91
  22.4 1.4 copy-start.3
  22.4 7.3 %copy-start.8 = (bf16[3,128]{1,0:T(4,128)(2,1)S(1)}, bf16[3,128]{1,0:T(4,128)(2,1)}, u32[]{:S(2)}) copy-start(bf16[3,128]{1,0:T(4,128)(2,1)} %param.19) | copy-start | bytes 2308
  24.0 1.2 copy-start.1
  25.2 25.9 %collective-permute-start = (bf16[512,384]{1,0:T(8,128)(2,1)S(1)}, bf16[512,384]{1,0:T(8,128)(2,1)S(1)}, u32[]{:S(2)}, u32[]{:S(2)}) collective-permute-start(bf16[512,384]{1,0:T(8,128)(2,1)S(1)} %constant_dynamic-slice_fusion.1), channel_id=1, source_target_pairs={{0,4},{1,5},{2,6},{3,7},{4,0},{5,1},{6,2},{7,3},{8,12},{9,13},{10,... | collective-permute-start | bytes 1179656 | tf_op jit(solution)/shard_map/ppermute | solution.py:42
  29.4 21.7 %collective-permute-start.1 = (bf16[32,2048]{1,0:T(8,128)(2,1)}, bf16[32,2048]{1,0:T(8,128)(2,1)}, u32[]{:S(2)}, u32[]{:S(2)}) collective-permute-start(bf16[32,2048]{1,0:T(8,128)(2,1)} %constant_dynamic-slice_fusion), channel_id=1, source_target_pairs={{0,4},{1,5},{2,6},{3,7},{4,0},{5,1},{6,2},{7,3},{8,12},{9,13},{10,... | collective-permute-start | bytes 393224 | tf_op jit(solution)/shard_map/ppermute | solution.py:42
  29.8 21.4 %collective-permute-start.2 = (bf16[3,128]{1,0:T(4,128)(2,1)S(1)}, bf16[3,128]{1,0:T(4,128)(2,1)S(1)}, u32[]{:S(2)}, u32[]{:S(2)}) collective-permute-start(bf16[3,128]{1,0:T(4,128)(2,1)S(1)} %copy-done.8), channel_id=1, source_target_pairs={{0,4},{1,5},{2,6},{3,7},{4,0},{5,1},{6,2},{7,3},{8,12},{9,13},{10,... | collective-permute-start | bytes 2312 | tf_op jit(solution)/shard_map/ppermute | solution.py:60
  54.6 83.1 %reduce-scatter.3.cloned.1.call-start = ((), (), s32[]{:S(2)}) async-start(), calls=%async_computation.6 | async-start | bytes 2621440 | tf_op jit(solution)/shard_map/reduce_scatter | solution.py:127
  54.7 32.8 %collective-permute-start.9 = (bf16[32,2048]{1,0:T(8,128)(2,1)}, bf16[32,2048]{1,0:T(8,128)(2,1)S(1)}, u32[]{:S(2)}, u32[]{:S(2)}) collective-permute-start(bf16[32,2048]{1,0:T(8,128)(2,1)} %collective-permute-done.1), channel_id=1, source_target_pairs={{0,24},{8,16},{16,8},{24,0},{1,25},{9,17},{17,9},{25,1},{2,26},{10... | collective-permute-start | bytes 393224 | tf_op jit(solution)/shard_map/ppermute | solution.py:52
  57.2 9.5 %collective-permute-start.8 = (bf16[32,2048]{1,0:T(8,128)(2,1)}, bf16[32,2048]{1,0:T(8,128)(2,1)S(1)}, u32[]{:S(2)}, u32[]{:S(2)}) collective-permute-start(bf16[32,2048]{1,0:T(8,128)(2,1)} %collective-permute-done.1), channel_id=1, source_target_pairs={{0,16},{8,24},{16,0},{24,8},{1,17},{9,25},{17,1},{25,9},{2,18},{10... | collective-permute-start | bytes 393224 | tf_op jit(solution)/shard_map/ppermute | solution.py:52
  57.7 8.0 %collective-permute-start.7 = (bf16[32,2048]{1,0:T(8,128)(2,1)}, bf16[32,2048]{1,0:T(8,128)(2,1)S(1)}, u32[]{:S(2)}, u32[]{:S(2)}) collective-permute-start(bf16[32,2048]{1,0:T(8,128)(2,1)} %collective-permute-done.1), channel_id=1, source_target_pairs={{0,8},{8,0},{16,24},{24,16},{1,9},{9,1},{17,25},{25,17},{2,10},{10... | collective-permute-start | bytes 393224 | tf_op jit(solution)/shard_map/ppermute | solution.py:52
  58.3 23.5 %collective-permute-start.5 = (bf16[512,384]{1,0:T(8,128)(2,1)S(1)}, bf16[512,384]{1,0:T(8,128)(2,1)S(1)}, u32[]{:S(2)}, u32[]{:S(2)}) collective-permute-start(bf16[512,384]{1,0:T(8,128)(2,1)S(1)} %collective-permute-done), channel_id=1, source_target_pairs={{0,24},{8,16},{16,8},{24,0},{1,25},{9,17},{17,9},{25,1},{2,26},{10... | collective-permute-start | bytes 1179656 | tf_op jit(solution)/shard_map/ppermute | solution.py:52
  60.7 21.1 %collective-permute-start.4 = (bf16[512,384]{1,0:T(8,128)(2,1)S(1)}, bf16[512,384]{1,0:T(8,128)(2,1)S(1)}, u32[]{:S(2)}, u32[]{:S(2)}) collective-permute-start(bf16[512,384]{1,0:T(8,128)(2,1)S(1)} %collective-permute-done), channel_id=1, source_target_pairs={{0,16},{8,24},{16,0},{24,8},{1,17},{9,25},{17,1},{25,9},{2,18},{10... | collective-permute-start | bytes 1179656 | tf_op jit(solution)/shard_map/ppermute | solution.py:52
  65.7 16.2 %copy-start.9 = (bf16[512,2048]{1,0:T(8,128)(2,1)S(1)}, bf16[512,2048]{1,0:T(8,128)(2,1)}, u32[]{:S(2)}) copy-start(bf16[512,2048]{1,0:T(8,128)(2,1)} %all-gather.3.cloned.1.call-done) | copy-start | bytes 6291460
  65.8 15.9 %collective-permute-start.3 = (bf16[512,384]{1,0:T(8,128)(2,1)S(1)}, bf16[512,384]{1,0:T(8,128)(2,1)S(1)}, u32[]{:S(2)}, u32[]{:S(2)}) collective-permute-start(bf16[512,384]{1,0:T(8,128)(2,1)S(1)} %collective-permute-done), channel_id=1, source_target_pairs={{0,8},{8,0},{16,24},{24,16},{1,9},{9,1},{17,25},{25,17},{2,10},{10... | collective-permute-start | bytes 1179656 | tf_op jit(solution)/shard_map/ppermute | solution.py:52
  82.9 8.2 %copy-start.5 = (bf16[128,2048]{1,0:T(8,128)(2,1)S(1)}, bf16[128,2048]{1,0:T(8,128)(2,1)}, u32[]{:S(2)}) copy-start(bf16[128,2048]{1,0:T(8,128)(2,1)} %param.20) | copy-start | bytes 1572868
  83.2 7.9 %collective-permute-start.6 = (bf16[2,256]{0,1:T(8,128)(2,1)S(1)}, bf16[2,256]{0,1:T(8,128)(2,1)S(1)}, u32[]{:S(2)}, u32[]{:S(2)}) collective-permute-start(bf16[2,256]{0,1:T(8,128)(2,1)S(1)} %pad_maximum_fusion.2), channel_id=1, source_target_pairs={{0,4},{1,5},{2,6},{3,7},{4,8},{5,9},{6,10},{7,11},{8,12},{9,13},{1... | collective-permute-start | bytes 3080 | tf_op jit(solution)/shard_map/ppermute | solution.py:113
  110.6 84.2 %reduce-scatter.5.cloned.1.call-start = ((), (), s32[]{:S(2)}) async-start(), calls=%async_computation.7 | async-start | bytes 5308416 | tf_op jit(solution)/shard_map/reduce_scatter | solution.py:138
  129.0 8.7 %copy-start.6 = (f32[64,2]{0,1:T(2,128)S(1)}, f32[64,2]{0,1:T(2,128)}, u32[]{:S(2)}) copy-start(f32[64,2]{0,1:T(2,128)} %param.24) | copy-start | bytes 1540
  137.7 62.8 %copy-start.4 = (s32[64,2]{1,0:T(8,128)S(1)}, s32[64,2]{1,0:T(8,128)}, u32[]{:S(2)}) copy-start(s32[64,2]{1,0:T(8,128)} %get-tuple-element.32) | copy-start | bytes 1540
  196.8 11.3 %all-to-all-start.1 = ((bf16[4,36,2048]{2,1,0:T(8,128)(2,1)}), bf16[4,36,2048]{2,1,0:T(8,128)(2,1)S(1)}, u32[]{:S(2)}, u32[]{:S(2)}) async-start(bf16[4,36,2048]{2,1,0:T(8,128)(2,1)} %reshape.86), calls=%async_computation.3 | async-start | bytes 1310720 | tf_op jit(solution)/shard_map/all_to_all | solution.py:139
Sparse Core Ops, SparseCore 0:
  14.4 40.1 all-gather.2
  56.3 54.2 all-gather.4
  113.4 24.2 reduce-scatter.2
  139.9 54.8 reduce-scatter.4

commit v2 on v1

--- a/solution.py
+++ b/solution.py
@@ -37,11 +37,9 @@
     joint = jnp.concatenate([gate_proj, conv_proj, value_proj], axis=1)
     swap = [(t, t ^ half) for t in range(n_tp)]
 
-    def own_piece(array):
+    def own_rows(array):
         rows = array.shape[0] // n_ep
-        return lax.ppermute(
-            lax.dynamic_slice_in_dim(array, ep_index * rows, rows, 0), "tp", swap
-        )
+        return lax.dynamic_slice_in_dim(array, ep_index * rows, rows, 0)
 
     def assembled(piece, array):
         rows = array.shape[0] // n_ep
@@ -55,13 +53,17 @@
             )
         return whole
 
-    joint_piece = own_piece(joint)
-    out_piece = own_piece(out_proj)
+    joint_rows = jnp.concatenate(
+        [own_rows(array) for array in (gate_proj, conv_proj, value_proj)], axis=1
+    )
+    joint_rows, out_rows, moe_tokens = lax.optimization_barrier(
+        (joint_rows, own_rows(out_proj), moe_tokens)
+    )
+    joint_piece = lax.ppermute(joint_rows, "tp", swap)
+    out_piece = lax.ppermute(out_rows, "tp", swap)
     other_taps = lax.ppermute(conv_taps, "tp", swap)
     normed = scaled_norm(mix_tokens, mix_gain)
     moe_normed = scaled_norm(moe_tokens, moe_gain)
-    normed, moe_normed = lax.optimization_barrier((normed, moe_normed))
-    gathered = lax.all_gather(normed, "tp", axis=0, tiled=True, axis_index_groups=halves)
     experts = expert_gate.shape[0] * lax.axis_size("ep")
     row_count, top_count = expert_ids.shape
     capacity = top_count * row_count // experts + max(1, top_count * row_count // (8 * experts))
@@ -85,12 +87,24 @@
         tiled=True,
     )
     arrived_rows = arrived.reshape(-1, width_model)
-    arrived_rows, gathered, joint_piece, out_piece, other_taps = lax.optimization_barrier(
-        (arrived_rows, gathered, joint_piece, out_piece, other_taps)
+    arrived_rows, joint_piece, out_piece, other_taps = lax.optimization_barrier(
+        (arrived_rows, joint_piece, out_piece, other_taps)
     )
     portion = lax.all_gather(arrived_rows, "tp", axis=0, tiled=True)
     other_joint = assembled(joint_piece, joint)
     other_out = assembled(out_piece, out_proj)
+    portion, other_joint, other_out, other_taps, joint = lax.optimization_barrier(
+        (portion, other_joint, other_out, other_taps, joint)
+    )
+    gathered = lax.all_gather(normed, "tp", axis=0, tiled=True, axis_index_groups=halves)
+    w_gate = expert_gate[0]
+    w_up = expert_up[0]
+    w_down = expert_down[0]
+    gate_value = jnp.dot(portion, w_gate, preferred_element_type=jnp.float32)
+    up_value = jnp.dot(portion, w_up, preferred_element_type=jnp.float32)
+    hidden = (jax.nn.silu(gate_value) * up_value).astype(jnp.bfloat16)
+    moe_partial = jnp.dot(hidden, w_down, preferred_element_type=jnp.float32).astype(jnp.bfloat16)
+    gathered, _ = lax.optimization_barrier((gathered, moe_partial))
     own_values = jnp.dot(gathered, joint, preferred_element_type=jnp.float32).astype(jnp.bfloat16)
     other_values = jnp.dot(gathered, other_joint, preferred_element_type=jnp.float32).astype(
         jnp.bfloat16
@@ -123,19 +137,11 @@
     mix_partial = jnp.dot(carried, out_weights, preferred_element_type=jnp.float32).astype(
         jnp.bfloat16
     )
-    portion, mix_partial = lax.optimization_barrier((portion, mix_partial))
+    summed = lax.psum_scatter(moe_partial, "tp", scatter_dimension=0, tiled=True)
+    mix_partial, summed = lax.optimization_barrier((mix_partial, summed))
     mix_out = lax.psum_scatter(
         mix_partial, "tp", scatter_dimension=0, tiled=True, axis_index_groups=halves
     )
-    w_gate = expert_gate[0]
-    w_up = expert_up[0]
-    w_down = expert_down[0]
-    gate_value = jnp.dot(portion, w_gate, preferred_element_type=jnp.float32)
-    up_value = jnp.dot(portion, w_up, preferred_element_type=jnp.float32)
-    hidden = (jax.nn.silu(gate_value) * up_value).astype(jnp.bfloat16)
-    moe_partial = jnp.dot(hidden, w_down, preferred_element_type=jnp.float32).astype(jnp.bfloat16)
-    moe_partial, mix_out = lax.optimization_barrier((moe_partial, mix_out))
-    summed = lax.psum_scatter(moe_partial, "tp", scatter_dimension=0, tiled=True)
     returned = lax.all_to_all(
         summed.reshape(experts, capacity, width_model),
         "ep",
@@ -170,4 +176,5 @@
         P("ep", "tp", None),
     )
     out_specs = (P(("ep", "tp"), None), P(("ep", "tp"), None))
+
     return jax.shard_map(shards, mesh=mesh, in_specs=in_specs, out_specs=out_specs, check_vma=False)

time: 221 us -> 219 us (level)
  waiting for transfers between devices: 130 us -> 126 us
  local copies, waits for them, and re-layouts: 14.1 us -> 16.8 us
    reduce_scatter x1, waiting for transfers between devices: 57 us -> 42.2 us  [shards(): lax.psum_scatter(moe_partial, 'tp', scatter_dimension=0, tiled=True)]
    all_gather x1, waiting for transfers between devices: 3.5 us -> 8.65 us  [shards(): lax.all_gather(normed, 'tp', axis=0, tiled=True, axis_index_groups=halves)]
    all_gather x1, waiting for transfers between devices: 16.8 us -> 20.9 us  [shards(): portion = lax.all_gather(arrived_rows, 'tp', axis=0, tiled=True)]
    all_to_all x1, waiting for transfers between devices: 0.01 us -> 3.9 us  [shards(): lax.all_to_all(outgoing.reshape(experts, capacity, width_model), 'ep', sp...]
    concatenate x0 -> x2, other arithmetic: none -> 3.34 us  [the longest x1 2.55 us: shards(): joint = jnp.concatenate([gate_proj, conv_proj, value_proj], axis=1)]
    ppermute x1, waiting for transfers between devices: 17.8 us -> 15.6 us  [shards(): other_taps = lax.ppermute(conv_taps, 'tp', swap)]
  transfers between devices with their start and end apart: 16 -> 16, of which waited for: 8 -> 11; matrix products, arithmetic and copies ran while one was open for 15% -> 20% of each run, Pallas kernels for 0% -> 0%
where the time goes in v2:
time: 219 us
  waiting for transfers between devices  126 us (58%)
  matrix products  27 us (12%)
  starting transfers between devices  25.9 us (12%)
  local copies, waits for them, and re-layouts  16.8 us (8%)
  between operations  14.2 us (6%)
  other arithmetic  9.21 us (4%)
    reduce_scatter x1, waiting for transfers between devices, shards(): lax.psum_scatter(moe_partial, 'tp', scatter_dimension=0, tiled=True)  42.2 us
    all_gather x1, waiting for transfers between devices, shards(): portion = lax.all_gather(arrived_rows, 'tp', axis=0, tiled=True)  20.9 us
    ppermute x1, waiting for transfers between devices, shards(): other_taps = lax.ppermute(conv_taps, 'tp', swap)  15.6 us
    ppermute x6, waiting for transfers between devices, assembled(): arrived_piece = lax.ppermute(piece, 'ep', [(e, e ^ k) for e in range(n_ep)])  15.1 us
    dot_general x1, matrix products, shards(): jnp.dot(hidden, w_down, preferred_element_type=jnp.float32)  11.4 us
    all_gather x1, waiting for transfers between devices, shards(): lax.all_gather(normed, 'tp', axis=0, tiled=True, axis_index_groups=halves)  8.65 us
    reduce_scatter x1, waiting for transfers between devices, shards(): lax.psum_scatter(mix_partial, 'tp', scatter_dimension=0, tiled=True, axis...  8.19 us
    all_to_all x1, waiting for transfers between devices, shards(): lax.all_to_all(summed.reshape(experts, capacity, width_model), 'ep', spli...  7.56 us
  transfers between devices with their start and end apart: 16, of which 11 were waited for; matrix products, arithmetic and copies ran while one was open for 20% of the time, Pallas kernels for 0%

profile of v2, /device:TPU:0, one launch (start us, length us, event | category | flops | bytes accessed | tf_op | source)
XLA Modules:
  0.0 218.8 jit_solution(681307983656228883)
XLA Ops:
  7.2 1.1 constant_dynamic-slice_fusion.3
  11.0 1.1 fusion.13
  15.2 5.2 %all-to-all-start = ((bf16[4,36,2048]{2,1,0:T(8,128)(2,1)}), bf16[4,36,2048]{2,1,0:T(8,128)(2,1)S(1)}, u32[]{:S(2)}, u32[]{:S(2)}) async-start(bf16[4,36,2048]{2,1,0:T(8,128)(2,1)} %reshape.84), calls=%async_computation | async-start | bytes 1310720 | tf_op jit(solution)/shard_map/all_to_all | solution.py:82
  20.4 2.6 %collective-permute-start = (bf16[512,384]{1,0:T(8,128)(2,1)}, bf16[512,384]{1,0:T(8,128)(2,1)}, u32[]{:S(2)}, u32[]{:S(2)}) collective-permute-start(bf16[512,384]{1,0:T(8,128)(2,1)} %pad_maximum_fusion.1), channel_id=1, source_target_pairs={{0,4},{1,5},{2,6},{3,7},{4,0},{5,1},{6,2},{7,3},{8,12},{9,13},{10,... | collective-permute-start | bytes 1179656 | tf_op jit(solution)/shard_map/ppermute | solution.py:62
  23.3 2.6 %collective-permute-start.2 = (bf16[3,128]{1,0:T(4,128)(2,1)S(1)}, bf16[3,128]{1,0:T(4,128)(2,1)S(1)}, u32[]{:S(2)}, u32[]{:S(2)}) collective-permute-start(bf16[3,128]{1,0:T(4,128)(2,1)S(1)} %copy-done.11), channel_id=1, source_target_pairs={{0,4},{1,5},{2,6},{3,7},{4,0},{5,1},{6,2},{7,3},{8,12},{9,13},{10,... | collective-permute-start | bytes 2312 | tf_op jit(solution)/shard_map/ppermute | solution.py:64
  25.9 3.9 %all-to-all-done = bf16[4,36,2048]{2,1,0:T(8,128)(2,1)S(1)} async-done(((bf16[4,36,2048]{2,1,0:T(8,128)(2,1)}), bf16[4,36,2048]{2,1,0:T(8,128)(2,1)S(1)}, u32[]{:S(2)}, u32[]{:S(2)}) %all-to-all-start) | async-done | bytes 589856 | tf_op jit(solution)/shard_map/all_to_all | solution.py:82
  30.7 15.6 %collective-permute-done.2 = bf16[3,128]{1,0:T(4,128)(2,1)S(1)} collective-permute-done((bf16[3,128]{1,0:T(4,128)(2,1)S(1)}, bf16[3,128]{1,0:T(4,128)(2,1)S(1)}, u32[]{:S(2)}, u32[]{:S(2)}) %collective-permute-start.2) | collective-permute-done | bytes 800 | tf_op jit(solution)/shard_map/ppermute | solution.py:64
  47.7 2.5 %pad_maximum_fusion = bf16[2048,384]{1,0:T(8,128)(2,1)} fusion(bf16[2048,128]{1,0:T(8,128)(2,1)S(1)} %copy-done.3, bf16[2048,128]{1,0:T(8,128)(2,1)} %param.17, bf16[2048,128]{1,0:T(8,128)(2,1)} %param.16), kind=kLoop, calls=%fused_computation.10 | loop fusion | flops 4718592 | bytes 3145728 | tf_op jit(solution)/shard_map/concatenate | solution.py:37
  50.3 1.6 collective-permute-start.6
  51.9 1.5 collective-permute-start.7
  53.8 1.6 collective-permute-start.3
  55.4 1.5 collective-permute-start.4
  56.9 1.3 broadcast_in_dim.4
  58.2 1.8 constant_dynamic-update-slice_fusion.7
  60.7 7.4 %collective-permute-done.3 = bf16[512,384]{1,0:T(8,128)(2,1)S(1)} collective-permute-done((bf16[512,384]{1,0:T(8,128)(2,1)}, bf16[512,384]{1,0:T(8,128)(2,1)S(1)}, u32[]{:S(2)}, u32[]{:S(2)}) %collective-permute-start.3) | collective-permute-done | bytes 393248 | tf_op jit(solution)/shard_map/ppermute | solution.py:50
  69.0 7.5 %collective-permute-done.4 = bf16[512,384]{1,0:T(8,128)(2,1)S(1)} collective-permute-done((bf16[512,384]{1,0:T(8,128)(2,1)}, bf16[512,384]{1,0:T(8,128)(2,1)S(1)}, u32[]{:S(2)}, u32[]{:S(2)}) %collective-permute-start.4) | collective-permute-done | bytes 393248 | tf_op jit(solution)/shard_map/ppermute | solution.py:50
  78.0 20.9 %all-gather.5.cloned.1.call-done = bf16[1152,2048]{1,0:T(8,128)(2,1)} async-done(((bf16[144,2048]{1,0:T(8,128)(2,1)}), bf16[1152,2048]{1,0:T(8,128)(2,1)}) %all-gather.5.cloned.1.call-update) | async-done | bytes 4718608 | tf_op jit(solution)/shard_map/all_gather | solution.py:93
  98.9 7.0 %fusion.3 = f32[1152,512]{1,0:T(8,128)} fusion(bf16[1152,2048]{1,0:T(8,128)(2,1)} %all-gather.5.cloned.1.call-done, bf16[1,2048,512]{2,1,0:T(8,128)(2,1)} %param.25), kind=kOutput, calls=%fused_computation.8 | convolution fusion | flops 2415919104 | bytes 9175040 | tf_op jit(solution)/shard_map/dot_general | solution.py:103
  106.0 11.4 %convolution_convert_fusion = bf16[1152,2048]{1,0:T(8,128)(2,1)} fusion(bf16[1,512,2048]{2,1,0:T(8,128)(2,1)S(1)} %copy-done, bf16[1152,2048]{1,0:T(8,128)(2,1)} %all-gather.5.cloned.1.call-done, f32[1152,512]{1,0:T(8,128)} %fusion.3, bf16[1,2048,512]{2,1,0:T(8,128)(2,1)} %param.26), kind=kOutput, calls=%fused_computation.1 | convolution fusion | flops 4837736448 | bytes 15990784 | tf_op jit(solution)/shard_map/dot_general | solution.py:106
  117.4 8.7 %all-gather.3.cloned.1.call-done = bf16[512,2048]{1,0:T(8,128)(2,1)} async-done(((bf16[128,2048]{1,0:T(8,128)(2,1)}), bf16[512,2048]{1,0:T(8,128)(2,1)}) %all-gather.3.cloned.1.call-update) | async-done | bytes 2097168 | tf_op jit(solution)/shard_map/all_gather | solution.py:99
  126.1 3.2 %convolution_convert_fusion.4 = bf16[512,384]{0,1:T(8,128)(2,1)S(1)} fusion(bf16[512,2048]{1,0:T(8,128)(2,1)} %all-gather.3.cloned.1.call-done, bf16[2048,384]{1,0:T(8,128)(2,1)} %pad_maximum_fusion), kind=kOutput, calls=%fused_computation.14 | convolution fusion | flops 805502976 | bytes 4063232 | tf_op jit(solution)/shard_map/dot_general | solution.py:108
  129.4 2.5 %convolution_convert_fusion.3 = bf16[512,384]{0,1:T(8,128)(2,1)S(1)} fusion(bf16[512,2048]{1,0:T(8,128)(2,1)S(1)} %copy-done.12, bf16[2048,384]{1,0:T(8,128)(2,1)} %constant_dynamic-update-slice_fusion.4), kind=kOutput, calls=%fused_computation.13 | convolution fusion | flops 805502976 | bytes 4063232 | tf_op jit(solution)/shard_map/dot_general | solution.py:109
  132.1 4.5 %collective-permute-start.9 = (bf16[2,256]{0,1:T(8,128)(2,1)S(1)}, bf16[2,256]{0,1:T(8,128)(2,1)S(1)}, u32[]{:S(2)}, u32[]{:S(2)}) collective-permute-start(bf16[2,256]{0,1:T(8,128)(2,1)S(1)} %pad_maximum_fusion.4), channel_id=1, source_target_pairs={{0,4},{1,5},{2,6},{3,7},{4,8},{5,9},{6,10},{7,11},{8,12},{9,13},{1... | collective-permute-start | bytes 3080 | tf_op jit(solution)/shard_map/ppermute | solution.py:127
  136.6 3.6 %collective-permute-done.9 = bf16[2,256]{0,1:T(8,128)(2,1)S(1)} collective-permute-done((bf16[2,256]{0,1:T(8,128)(2,1)S(1)}, bf16[2,256]{0,1:T(8,128)(2,1)S(1)}, u32[]{:S(2)}, u32[]{:S(2)}) %collective-permute-start.9) | collective-permute-done | bytes 1056 | tf_op jit(solution)/shard_map/ppermute | solution.py:127
  140.2 2.5 %convolution_convert_fusion.1 = bf16[512,2048]{1,0:T(8,128)(2,1)} fusion(bf16[128,2048]{1,0:T(8,128)(2,1)S(1)} %constant_dynamic-update-slice_fusion, bf16[128,2048]{1,0:T(8,128)(2,1)S(1)} %copy-done.6, bf16[512,256]{0,1:T(8,128)(2,1)S(1)} %multiply_convert_fusion.1, bf16[2,256]{0,1:T(8,128)(2,1)S(1)} %collective-permute-done.9, ...), kind=kOutput, calls=%fused_computation.3 | convolution fusion | flops 542638080 | bytes 3674112 | tf_op jit(solution)/shard_map/dot_general | solution.py:137
  142.7 42.2 %reduce-scatter.3.cloned.1.call-done = bf16[144,2048]{1,0:T(8,128)(2,1)} async-done(((bf16[1152,2048]{1,0:T(8,128)(2,1)}), bf16[144,2048]{1,0:T(8,128)(2,1)}) %reduce-scatter.3.cloned.1.call-update) | async-done | bytes 589840 | tf_op jit(solution)/shard_map/reduce_scatter | solution.py:140
  187.0 3.5 %all-to-all-start.1 = ((bf16[4,36,2048]{2,1,0:T(8,128)(2,1)}), bf16[4,36,2048]{2,1,0:T(8,128)(2,1)S(1)}, u32[]{:S(2)}, u32[]{:S(2)}) async-start(bf16[4,36,2048]{2,1,0:T(8,128)(2,1)} %reshape.86), calls=%async_computation.3 | async-start | bytes 1310720 | tf_op jit(solution)/shard_map/all_to_all | solution.py:145
  190.7 7.6 %all-to-all-done.1 = bf16[4,36,2048]{2,1,0:T(8,128)(2,1)S(1)} async-done(((bf16[4,36,2048]{2,1,0:T(8,128)(2,1)}), bf16[4,36,2048]{2,1,0:T(8,128)(2,1)S(1)}, u32[]{:S(2)}, u32[]{:S(2)}) %all-to-all-start.1) | async-done | bytes 589856 | tf_op jit(solution)/shard_map/all_to_all | solution.py:145
  198.4 1.7 gather_fusion
  200.1 1.7 reshape.88
  201.8 2.2 %multiply_reduce_fusion = bf16[64,2048]{1,0:T(8,128)(2,1)} fusion(f32[64,2,2048]{2,1,0:T(2,128)S(1)} %reshape.88, f32[64,2]{1,0:T(8,128)S(1)} %copy.31), kind=kLoop, calls=%fused_computation.21 | loop fusion | flops 393216 | bytes 1311232 | tf_op jit(solution)/shard_map/reduce_sum | solution.py:155
  204.1 8.2 %reduce-scatter.5.cloned.1.call-done = bf16[128,2048]{1,0:T(8,128)(2,1)} async-done(((bf16[512,2048]{1,0:T(8,128)(2,1)}), bf16[128,2048]{1,0:T(8,128)(2,1)}) %reduce-scatter.5.cloned.1.call-update) | async-done | bytes 524304 | tf_op jit(solution)/shard_map/reduce_scatter | solution.py:142
  (87 shorter events, 14.5 us)
Async XLA Ops:
  7.2 98.8 %copy-start = (bf16[1,512,2048]{2,1,0:T(8,128)(2,1)S(1)}, bf16[1,512,2048]{2,1,0:T(8,128)(2,1)}, u32[]{:S(2)}) copy-start(bf16[1,512,2048]{2,1,0:T(8,128)(2,1)} %param.27) | copy-start | bytes 6291460
  7.2 6.6 %copy-start.2 = (bf16[64,2048]{1,0:T(8,128)(2,1)S(1)}, bf16[64,2048]{1,0:T(8,128)(2,1)}, u32[]{:S(2)}) copy-start(bf16[64,2048]{1,0:T(8,128)(2,1)} %param.21) | copy-start | bytes 786436
  7.2 5.0 %copy-start.10 = (s32[64,2]{0,1:T(2,128)S(1)}, s32[64,2]{0,1:T(2,128)}, u32[]{:S(2)}) copy-start(s32[64,2]{0,1:T(2,128)} %param.23) | copy-start | bytes 1540
  7.2 6.6 %copy-start.8 = (bf16[2048]{0:T(1024)(128)(2,1)S(1)}, bf16[2048]{0:T(1024)(128)(2,1)}, u32[]{:S(2)}) copy-start(bf16[2048]{0:T(1024)(128)(2,1)} %param.22) | copy-start | bytes 12292
  11.0 12.3 %copy-start.11 = (bf16[3,128]{1,0:T(4,128)(2,1)S(1)}, bf16[3,128]{1,0:T(4,128)(2,1)}, u32[]{:S(2)}) copy-start(bf16[3,128]{1,0:T(4,128)(2,1)} %param.19) | copy-start | bytes 2308
  14.2 32.2 %copy-start.9 = (bf16[2048]{0:T(1024)(128)(2,1)S(1)}, bf16[2048]{0:T(1024)(128)(2,1)}, u32[]{:S(2)}) copy-start(bf16[2048]{0:T(1024)(128)(2,1)} %param.15) | copy-start | bytes 12292
  14.2 32.2 %copy-start.1 = (bf16[128,2048]{1,0:T(8,128)(2,1)S(1)}, bf16[128,2048]{1,0:T(8,128)(2,1)}, u32[]{:S(2)}) copy-start(bf16[128,2048]{1,0:T(8,128)(2,1)} %param.14) | copy-start | bytes 1572868
  15.2 14.6 %all-to-all-start = ((bf16[4,36,2048]{2,1,0:T(8,128)(2,1)}), bf16[4,36,2048]{2,1,0:T(8,128)(2,1)S(1)}, u32[]{:S(2)}, u32[]{:S(2)}) async-start(bf16[4,36,2048]{2,1,0:T(8,128)(2,1)} %reshape.84), calls=%async_computation | async-start | bytes 1310720 | tf_op jit(solution)/shard_map/all_to_all | solution.py:82
  20.4 78.6 %all-gather.5.cloned.1.call-start = ((), (), s32[]{:S(2)}) async-start(), calls=%async_computation.5 | async-start | bytes 5308416 | tf_op jit(solution)/shard_map/all_gather | solution.py:93
  20.4 25.9 %collective-permute-start = (bf16[512,384]{1,0:T(8,128)(2,1)}, bf16[512,384]{1,0:T(8,128)(2,1)}, u32[]{:S(2)}, u32[]{:S(2)}) collective-permute-start(bf16[512,384]{1,0:T(8,128)(2,1)} %pad_maximum_fusion.1), channel_id=1, source_target_pairs={{0,4},{1,5},{2,6},{3,7},{4,0},{5,1},{6,2},{7,3},{8,12},{9,13},{10,... | collective-permute-start | bytes 1179656 | tf_op jit(solution)/shard_map/ppermute | solution.py:62
  23.0 23.3 %collective-permute-start.1 = (bf16[32,2048]{1,0:T(8,128)(2,1)S(1)}, bf16[32,2048]{1,0:T(8,128)(2,1)S(1)}, u32[]{:S(2)}, u32[]{:S(2)}) collective-permute-start(bf16[32,2048]{1,0:T(8,128)(2,1)S(1)} %constant_dynamic-slice_fusion), channel_id=1, source_target_pairs={{0,4},{1,5},{2,6},{3,7},{4,0},{5,1},{6,2},{7,3},{8,12},{9,13},{10,... | collective-permute-start | bytes 393224 | tf_op jit(solution)/shard_map/ppermute | solution.py:63
  23.3 23.0 %collective-permute-start.2 = (bf16[3,128]{1,0:T(4,128)(2,1)S(1)}, bf16[3,128]{1,0:T(4,128)(2,1)S(1)}, u32[]{:S(2)}, u32[]{:S(2)}) collective-permute-start(bf16[3,128]{1,0:T(4,128)(2,1)S(1)} %copy-done.11), channel_id=1, source_target_pairs={{0,4},{1,5},{2,6},{3,7},{4,0},{5,1},{6,2},{7,3},{8,12},{9,13},{10,... | collective-permute-start | bytes 2312 | tf_op jit(solution)/shard_map/ppermute | solution.py:64
  30.7 17.0 %copy-start.3 = (bf16[2048,128]{1,0:T(8,128)(2,1)S(1)}, bf16[2048,128]{1,0:T(8,128)(2,1)}, u32[]{:S(2)}) copy-start(bf16[2048,128]{1,0:T(8,128)(2,1)} %param.18) | copy-start | bytes 1572868
  46.4 79.7 %all-gather.3.cloned.1.call-start = ((), (), s32[]{:S(2)}) async-start(), calls=%async_computation.4 | async-start | bytes 2621440 | tf_op jit(solution)/shard_map/all_gather | solution.py:99
  47.6 137.3 %reduce-scatter.3.cloned.1.call-start = ((), (), s32[]{:S(2)}) async-start(), calls=%async_computation.6 | async-start | bytes 5308416 | tf_op jit(solution)/shard_map/reduce_scatter | solution.py:140
  50.3 9.7 %collective-permute-start.6 = (bf16[32,2048]{1,0:T(8,128)(2,1)S(1)}, bf16[32,2048]{1,0:T(8,128)(2,1)S(1)}, u32[]{:S(2)}, u32[]{:S(2)}) collective-permute-start(bf16[32,2048]{1,0:T(8,128)(2,1)S(1)} %collective-permute-done.1), channel_id=1, source_target_pairs={{0,8},{8,0},{16,24},{24,16},{1,9},{9,1},{17,25},{25,17},{2,10},{10... | collective-permute-start | bytes 393224 | tf_op jit(solution)/shard_map/ppermute | solution.py:50
  51.9 8.8 %collective-permute-start.7 = (bf16[32,2048]{1,0:T(8,128)(2,1)S(1)}, bf16[32,2048]{1,0:T(8,128)(2,1)S(1)}, u32[]{:S(2)}, u32[]{:S(2)}) collective-permute-start(bf16[32,2048]{1,0:T(8,128)(2,1)S(1)} %collective-permute-done.1), channel_id=1, source_target_pairs={{0,16},{8,24},{16,0},{24,8},{1,17},{9,25},{17,1},{25,9},{2,18},{10... | collective-permute-start | bytes 393224 | tf_op jit(solution)/shard_map/ppermute | solution.py:50
  53.4 7.3 %collective-permute-start.8 = (bf16[32,2048]{1,0:T(8,128)(2,1)S(1)}, bf16[32,2048]{1,0:T(8,128)(2,1)S(1)}, u32[]{:S(2)}, u32[]{:S(2)}) collective-permute-start(bf16[32,2048]{1,0:T(8,128)(2,1)S(1)} %collective-permute-done.1), channel_id=1, source_target_pairs={{0,24},{8,16},{16,8},{24,0},{1,25},{9,17},{17,9},{25,1},{2,26},{10... | collective-permute-start | bytes 393224 | tf_op jit(solution)/shard_map/ppermute | solution.py:50
  53.8 14.4 %collective-permute-start.3 = (bf16[512,384]{1,0:T(8,128)(2,1)}, bf16[512,384]{1,0:T(8,128)(2,1)S(1)}, u32[]{:S(2)}, u32[]{:S(2)}) collective-permute-start(bf16[512,384]{1,0:T(8,128)(2,1)} %collective-permute-done), channel_id=1, source_target_pairs={{0,8},{8,0},{16,24},{24,16},{1,9},{9,1},{17,25},{25,17},{2,10},{10... | collective-permute-start | bytes 1179656 | tf_op jit(solution)/shard_map/ppermute | solution.py:50
  55.4 21.0 %collective-permute-start.4 = (bf16[512,384]{1,0:T(8,128)(2,1)}, bf16[512,384]{1,0:T(8,128)(2,1)S(1)}, u32[]{:S(2)}, u32[]{:S(2)}) collective-permute-start(bf16[512,384]{1,0:T(8,128)(2,1)} %collective-permute-done), channel_id=1, source_target_pairs={{0,16},{8,24},{16,0},{24,8},{1,17},{9,25},{17,1},{25,9},{2,18},{10... | collective-permute-start | bytes 1179656 | tf_op jit(solution)/shard_map/ppermute | solution.py:50
  60.0 17.2 %collective-permute-start.5 = (bf16[512,384]{1,0:T(8,128)(2,1)}, bf16[512,384]{1,0:T(8,128)(2,1)S(1)}, u32[]{:S(2)}, u32[]{:S(2)}) collective-permute-start(bf16[512,384]{1,0:T(8,128)(2,1)} %collective-permute-done), channel_id=1, source_target_pairs={{0,24},{8,16},{16,8},{24,0},{1,25},{9,17},{17,9},{25,1},{2,26},{10... | collective-permute-start | bytes 1179656 | tf_op jit(solution)/shard_map/ppermute | solution.py:50
  117.4 94.9 %reduce-scatter.5.cloned.1.call-start = ((), (), s32[]{:S(2)}) async-start(), calls=%async_computation.7 | async-start | bytes 2621440 | tf_op jit(solution)/shard_map/reduce_scatter | solution.py:142
  126.1 3.3 %copy-start.12 = (bf16[512,2048]{1,0:T(8,128)(2,1)S(1)}, bf16[512,2048]{1,0:T(8,128)(2,1)}, u32[]{:S(2)}) copy-start(bf16[512,2048]{1,0:T(8,128)(2,1)} %all-gather.3.cloned.1.call-done) | copy-start | bytes 6291460
  129.4 10.9 %copy-start.6 = (bf16[128,2048]{1,0:T(8,128)(2,1)S(1)}, bf16[128,2048]{1,0:T(8,128)(2,1)}, u32[]{:S(2)}) copy-start(bf16[128,2048]{1,0:T(8,128)(2,1)} %param.20) | copy-start | bytes 1572868
  132.1 8.1 %collective-permute-start.9 = (bf16[2,256]{0,1:T(8,128)(2,1)S(1)}, bf16[2,256]{0,1:T(8,128)(2,1)S(1)}, u32[]{:S(2)}, u32[]{:S(2)}) collective-permute-start(bf16[2,256]{0,1:T(8,128)(2,1)S(1)} %pad_maximum_fusion.4), channel_id=1, source_target_pairs={{0,4},{1,5},{2,6},{3,7},{4,8},{5,9},{6,10},{7,11},{8,12},{9,13},{1... | collective-permute-start | bytes 3080 | tf_op jit(solution)/shard_map/ppermute | solution.py:127
  142.7 42.2 %copy-start.7 = (f32[64,2]{0,1:T(2,128)S(1)}, f32[64,2]{0,1:T(2,128)}, u32[]{:S(2)}) copy-start(f32[64,2]{0,1:T(2,128)} %param.24) | copy-start | bytes 1540
  142.7 47.7 %copy-start.5 = (s32[64,2]{1,0:T(8,128)S(1)}, s32[64,2]{1,0:T(8,128)}, u32[]{:S(2)}) copy-start(s32[64,2]{1,0:T(8,128)} %get-tuple-element.40) | copy-start | bytes 1540
  185.0 1.1 copy-start.4
  187.0 11.3 %all-to-all-start.1 = ((bf16[4,36,2048]{2,1,0:T(8,128)(2,1)}), bf16[4,36,2048]{2,1,0:T(8,128)(2,1)S(1)}, u32[]{:S(2)}, u32[]{:S(2)}) async-start(bf16[4,36,2048]{2,1,0:T(8,128)(2,1)} %reshape.86), calls=%async_computation.3 | async-start | bytes 1310720 | tf_op jit(solution)/shard_map/all_to_all | solution.py:145
Sparse Core Ops, SparseCore 0:
  46.5 52.4 all-gather.4
  101.1 24.9 all-gather.2
  128.4 56.5 reduce-scatter.2
  187.7 24.5 reduce-scatter.4
